TPU v7x, 32 devices: a whole 2x2x4 slice. The times are simulated.
32 devices in a mesh: ep: 4 (over z), tp: 8 (over y, x, core).
Axes of the slice: x: 2, y: 2, z: 4, core: 2. Of those that a mesh axis runs over, the one named last changes fastest.
Arguments:
- hidden: bfloat16 [64, 4096], P('ep', 'tp'), may hold values from -6 to 6
- norm_gain: float32 [4096], replicated, may hold values from 0.1 to 1.9
- routes: int32 [64, 4], P('ep'), may hold values from 0 to 7, all different within a row; in each aligned block of 16 rows (0 to 15, 16 to 31, ...) at most 13 rows name the same one
- route_weights: float32 [64, 4], P('ep'), may hold values from 0.1 to 1
- gate_weight: bfloat16 [8, 1024, 4096], P('ep', 'tp'), may hold values from -0.09375 to 0.09375
- up_weight: bfloat16 [8, 1024, 4096], P('ep', 'tp'), may hold values from -0.09375 to 0.09375
- down_weight: bfloat16 [8, 1024, 4096], P('ep', 'tp'), may hold values from -0.25 to 0.25
- shared_gate: bfloat16 [1024, 4096], P('tp'), may hold values from -0.09375 to 0.09375
- shared_up: bfloat16 [1024, 4096], P('tp'), may hold values from -0.09375 to 0.09375
- shared_down: bfloat16 [1024, 4096], P('tp'), may hold values from -0.25 to 0.25
Outputs:
- mixed: bfloat16 [64, 4096], P('ep', 'tp')
Inputs may be any that keep to these rules, and one draw needn't show every extreme that they name: `routes`: each row names 4 different experts; among the rows of one index of ep (aligned blocks of 16 rows) no expert is named more than 13 times, a bound that some block reaches.
All inputs are finite; a program needn't handle non-finite values.
Results may differ from a plain program's by a relative error of at most 0.017.
Values may be sent and summed in bfloat16 or wider, within the bound.
A program may use at most 64 MiB of HBM per device.

v0:
```python
import jax
import jax.numpy as jnp
from jax import lax
from jax.sharding import PartitionSpec as P

norm_eps = 1e-06


def norm_rows(gathered, norm_gain):
    values = gathered.astype(jnp.float32)
    inv_scale = lax.rsqrt(jnp.mean(values * values, axis=-1, keepdims=True) + norm_eps)
    return (values * inv_scale * norm_gain).astype(jnp.bfloat16)


def slot_table(routes, expert_count, capacity):
    onehot = (
        routes[:, :, None] == jnp.arange(expert_count, dtype=jnp.int32)[None, None, :]
    ).astype(jnp.int32)
    used_mask = jnp.sum(onehot, axis=1)
    before = jnp.cumsum(used_mask, axis=0) - used_mask
    slot_rank = jnp.sum(onehot * before[:, None, :], axis=2)
    return routes * capacity + slot_rank


def per_device(
    hidden,
    norm_gain,
    routes,
    route_weights,
    gate_weight,
    up_weight,
    down_weight,
    shared_gate,
    shared_up,
    shared_down,
):
    width_group = lax.axis_size("tp")
    down_local = lax.all_to_all(down_weight, "tp", split_axis=2, concat_axis=1, tiled=True)
    gathered = lax.all_gather(hidden, "tp", axis=1, tiled=True)
    normed = norm_rows(gathered, norm_gain)
    tok_rows, top_count = routes.shape
    local_experts = gate_weight.shape[0]
    groups = lax.axis_size("ep")
    experts = local_experts * groups
    capacity = min(tok_rows, 3 * tok_rows * top_count // (2 * experts) + 1)
    full_width = gathered.shape[1]
    slot_ids = slot_table(routes, experts, capacity)
    slot_range = jnp.arange(experts * capacity, dtype=jnp.int32)
    matches = slot_ids[:, :, None] == slot_range[None, None, :]
    combine = jnp.sum(jnp.where(matches, route_weights[:, :, None], 0.0), axis=1)
    select = jnp.sum(
        (slot_range[:, None, None] == slot_ids[None, :, :]).astype(jnp.bfloat16), axis=2
    )
    packed = jnp.dot(select, normed, preferred_element_type=jnp.float32).astype(jnp.bfloat16)
    packed = packed.reshape(groups, local_experts, capacity, full_width)
    arrived = lax.all_to_all(packed, "ep", split_axis=0, concat_axis=0, tiled=True)
    gate_vals = jnp.einsum(
        "secd,efd->secf", arrived, gate_weight, preferred_element_type=jnp.float32
    )
    up_vals = jnp.einsum("secd,efd->secf", arrived, up_weight, preferred_element_type=jnp.float32)
    inner_vals = (jax.nn.silu(gate_vals) * up_vals).astype(jnp.bfloat16)
    dims = (((1,), (1,)), ((), ()))
    shared_gates = lax.dot_general(normed, shared_gate, dims, preferred_element_type=jnp.float32)
    shared_ups = lax.dot_general(normed, shared_up, dims, preferred_element_type=jnp.float32)
    shared_inner = (jax.nn.silu(shared_gates) * shared_ups).astype(jnp.bfloat16)
    shared_part = jnp.dot(shared_inner, shared_down, preferred_element_type=jnp.float32).astype(
        jnp.bfloat16
    )
    inner_whole = lax.all_gather(inner_vals, "tp", axis=3, tiled=True)
    slots, _, cap_rows, hidden_units = inner_whole.shape
    block_units = hidden_units // width_group
    inner_blocks = inner_whole.reshape(slots, local_experts, cap_rows, width_group, block_units)
    down_blocks = down_local.reshape(local_experts, width_group, block_units, down_local.shape[2])
    block_sums = jnp.einsum(
        "secpf,epfd->secpd", inner_blocks, down_blocks, preferred_element_type=jnp.float32
    ).astype(jnp.bfloat16)
    answers = jnp.sum(block_sums.astype(jnp.float32), axis=3).astype(jnp.bfloat16)
    shared_sum = lax.psum_scatter(shared_part, "tp", scatter_dimension=1, tiled=True).astype(
        jnp.float32
    )
    returned = lax.all_to_all(answers, "ep", split_axis=0, concat_axis=0, tiled=True)
    flat_rows = returned.reshape(-1, returned.shape[3]).astype(jnp.float32)
    routed = jnp.dot(combine, flat_rows, precision=lax.Precision.HIGHEST)
    return (routed + shared_sum).astype(jnp.bfloat16)


def solution(mesh):
    in_specs = (
        P("ep", "tp"),
        P(),
        P("ep", None),
        P("ep", None),
        P("ep", "tp", None),
        P("ep", "tp", None),
        P("ep", "tp", None),
        P("tp", None),
        P("tp", None),
        P("tp", None),
    )
    out_specs = P("ep", "tp")
    return jax.shard_map(
        per_device, mesh=mesh, in_specs=in_specs, out_specs=out_specs, check_vma=False
    )
```

profile of v0, /device:TPU:0, one launch (start us, length us, event | category | flops | bytes accessed | tf_op | source)
XLA Modules:
  0.0 113.9 jit_solution(8584589679115222297)
XLA Ops:
  6.5 0.0 copy-start
  6.5 0.8 convert_reduce_fusion
  7.4 0.1 copy.40
  7.5 0.1 copy.42
  7.6 0.7 select_reduce_fusion.1
  8.3 0.7 multiply_add_fusion
  9.0 0.1 fusion.33
  9.0 10.9 %all_gather.6 = bf16[16,4096]{1,0:T(8,128)(2,1)S(1)} all-gather(bf16[16,512]{1,0:T(8,128)(2,1)} %param.10), channel_id=1, replica_groups=mesh['ep'=4,'tp'=8] {'tp'}, dimensions={1}, use_global_device_ids=true | all-gather | bytes 147456 | tf_op jit(solution)/shard_map/all_gather | solution.py:39
  19.9 0.1 fusion.28
  20.1 2.1 %convolution_convert_fusion = bf16[104,4096]{1,0:T(8,128)(2,1)} fusion(bf16[104,16]{0,1:T(8,128)(2,1)S(1)} %fusion.33, bf16[16,4096]{1,0:T(8,128)(2,1)S(1)} %all_gather.6, f32[4096]{0:T(1024)} %param.11, f32[16]{0:T(128)S(1)} %add_rsqrt_fusion), kind=kOutput, calls=%fused_computation | convolution fusion | flops 14319616 | bytes 1002816 | tf_op jit(solution)/shard_map/dot_general | solution.py:54
  22.2 1.4 %reshape.33 = bf16[4,2,13,4096]{3,2,1,0:T(8,128)(2,1)S(1)} reshape(bf16[104,4096]{1,0:T(8,128)(2,1)} %convolution_convert_fusion) | data formatting | bytes 1703936 | tf_op jit(solution)/shard_map/reshape | solution.py:55
  23.6 1.8 %copy.43 = bf16[4,2,13,4096]{3,1,2,0:T(2,128)(2,1)} copy(bf16[4,2,13,4096]{3,2,1,0:T(8,128)(2,1)S(1)} %reshape.33) | data formatting | bytes 1703936 | tf_op jit(solution)/shard_map/reshape | solution.py:55
  25.4 4.9 %all-to-all-start = ((bf16[4,2,13,4096]{3,1,2,0:T(2,128)(2,1)}), bf16[4,2,13,4096]{3,1,2,0:T(2,128)(2,1)S(1)}, u32[]{:S(2)}, u32[]{:S(2)}) async-start(bf16[4,2,13,4096]{3,1,2,0:T(2,128)(2,1)} %copy.43), calls=%async_computation | async-start | bytes 1703936 | tf_op jit(solution)/shard_map/all_to_all | solution.py:56
  30.3 6.2 %copy.47 = bf16[2,128,4096]{1,0,2:T(2,128)(2,1)} copy(bf16[2,128,4096]{2,1,0:T(8,128)(2,1)} %param.16) | data formatting | bytes 4194304 | tf_op args[6]
  36.5 0.0 copy-start.2
  36.5 15.8 %all-to-all-done = bf16[4,2,13,4096]{3,1,2,0:T(2,128)(2,1)S(1)} async-done(((bf16[4,2,13,4096]{3,1,2,0:T(2,128)(2,1)}), bf16[4,2,13,4096]{3,1,2,0:T(2,128)(2,1)S(1)}, u32[]{:S(2)}, u32[]{:S(2)}) %all-to-all-start) | async-done | bytes 852000 | tf_op jit(solution)/shard_map/all_to_all | solution.py:56
  52.3 4.3 %all-to-all-start.1 = ((bf16[2,128,4096]{1,0,2:T(2,128)(2,1)}), bf16[2,128,4096]{1,0,2:T(2,128)(2,1)}, u32[]{:S(2)}, u32[]{:S(2)}) async-start(bf16[2,128,4096]{1,0,2:T(2,128)(2,1)} %copy.47), calls=%async_computation.1 | async-start | bytes 4194304 | tf_op jit(solution)/shard_map/all_to_all | solution.py:38
  56.7 0.0 reduce-scatter.2.cloned.1.call-start
  56.7 0.0 copy-done.2
  56.7 1.6 %fusion.43 = f32[16,128]{1,0:T(8,128)S(1)} fusion(bf16[128,4096]{1,0:T(8,128)(2,1)} %param.17, bf16[16,4096]{1,0:T(8,128)(2,1)S(1)} %all_gather.6, f32[4096]{0:T(1024)S(1)} %copy-done.2, f32[16]{0:T(128)S(1)} %add_rsqrt_fusion), kind=kOutput, calls=%fused_computation.43 | convolution fusion | flops 17039360 | bytes 1204288 | tf_op jit(solution)/shard_map/dot_general | solution.py:63
  58.4 3.1 %convolution_convert_fusion.1 = bf16[16,4096]{1,0:T(8,128)(2,1)} fusion(bf16[128,4096]{1,0:T(8,128)(2,1)} %param.19, bf16[128,4096]{1,0:T(8,128)(2,1)} %param.18, f32[16,128]{1,0:T(8,128)S(1)} %fusion.43, bf16[16,4096]{1,0:T(8,128)(2,1)S(1)} %all_gather.6, f32[4096]{0:T(1024)S(1)} %copy-done.2, f32[16]{0:T(128)S(1)} %add_rsqrt_fusion), kind=kOutput, calls=%fused_computation.1 | convolution fusion | flops 33894400 | bytes 2383936 | tf_op jit(solution)/shard_map/dot_general | solution.py:66
  61.5 0.0 reduce-scatter.2.cloned.1.call-update
  61.5 0.0 copy-done
  61.6 0.0 copy-start.1
  61.6 0.8 fusion.12
  62.4 0.7 copy-done.1
  63.1 0.9 fusion.21
  64.0 22.9 %all_gather.7 = bf16[4,2,13,1024]{3,2,0,1:T(8,128)(2,1)S(1)} all-gather(bf16[4,2,13,128]{3,2,0,1:T(8,128)(2,1)S(1)} %fusion.21), channel_id=1, replica_groups=mesh['ep'=4,'tp'=8] {'tp'}, dimensions={3}, use_global_device_ids=true | all-gather | bytes 239616 | tf_op jit(solution)/shard_map/all_gather | solution.py:69
  86.9 0.2 reshape.39
  87.1 0.0 all-to-all-done.1
  87.1 6.2 %copy.49 = bf16[2,128,8,512]{3,1,2,0:T(8,128)(2,1)} copy(bf16[2,128,8,512]{1,0,3,2:T(2,128)(2,1)} %bitcast.6) | data formatting | bytes 4194304 | tf_op jit(solution)/shard_map/all_to_all | solution.py:38
  93.2 0.0 copy-start.3
  93.2 2.1 %fusion.9 = bf16[2,4,13,512]{3,2,1,0:T(8,128)(2,1)S(1)} fusion(bf16[2,128,8,512]{3,1,2,0:T(8,128)(2,1)} %copy.49, bf16[4,2,13,8,128]{4,3,2,0,1:T(8,128)(2,1)S(1)} %reshape.39), kind=kOutput, calls=%fused_computation.9 | convolution fusion | flops 109850624 | bytes 2416640 | tf_op jit(solution)/shard_map/secpf,epfd->secpd/dot_general | solution.py:74
  95.3 0.8 copy.51
  96.1 3.3 %all-to-all-start.2 = ((bf16[4,2,13,512]{3,1,2,0:T(2,128)(2,1)}), bf16[4,2,13,512]{3,1,2,0:T(2,128)(2,1)S(1)}, u32[]{:S(2)}, u32[]{:S(2)}) async-start(bf16[4,2,13,512]{3,1,2,0:T(2,128)(2,1)} %copy.51), calls=%async_computation.2 | async-start | bytes 212992 | tf_op jit(solution)/shard_map/all_to_all | solution.py:81
  99.4 0.0 copy-done.3
  99.4 0.1 select_reduce_fusion
  99.5 6.0 %all-to-all-done.2 = bf16[4,2,13,512]{3,1,2,0:T(2,128)(2,1)S(1)} async-done(((bf16[4,2,13,512]{3,1,2,0:T(2,128)(2,1)}), bf16[4,2,13,512]{3,1,2,0:T(2,128)(2,1)S(1)}, u32[]{:S(2)}, u32[]{:S(2)}) %all-to-all-start.2) | async-done | bytes 106528 | tf_op jit(solution)/shard_map/all_to_all | solution.py:81
  105.5 0.1 reshape.35
  105.5 0.0 reduce-scatter.2.cloned.1.call-done
  105.6 1.5 %fusion.24 = bf16[16,512]{1,0:T(8,128)(2,1)} fusion(f32[16,104]{1,0:T(8,128)S(1)} %select_reduce_fusion, bf16[104,512]{1,0:T(8,128)(2,1)S(1)} %reshape.35, bf16[16,512]{1,0:T(8,128)(2,1)} %reduce-scatter.2.cloned.1.call-done), kind=kOutput, calls=%fused_computation.15 | convolution fusion | flops 10248192 | bytes 145920 | tf_op jit(solution)/shard_map/dot_general | solution.py:83
  (4 shorter events, 0.1 us)
Async XLA Ops:
  6.5 55.0 %copy-start = (bf16[2,128,4096]{2,1,0:T(8,128)(2,1)S(1)}, bf16[2,128,4096]{2,1,0:T(8,128)(2,1)}, u32[]{:S(2)}) copy-start(bf16[2,128,4096]{2,1,0:T(8,128)(2,1)} %param.14) | copy-start | bytes 6291460
  25.4 26.9 %all-to-all-start = ((bf16[4,2,13,4096]{3,1,2,0:T(2,128)(2,1)}), bf16[4,2,13,4096]{3,1,2,0:T(2,128)(2,1)S(1)}, u32[]{:S(2)}, u32[]{:S(2)}) async-start(bf16[4,2,13,4096]{3,1,2,0:T(2,128)(2,1)} %copy.43), calls=%async_computation | async-start | bytes 1703936 | tf_op jit(solution)/shard_map/all_to_all | solution.py:56
  36.5 20.2 %copy-start.2 = (f32[4096]{0:T(1024)S(1)}, f32[4096]{0:T(1024)}, u32[]{:S(2)}) copy-start(f32[4096]{0:T(1024)} %param.11) | copy-start | bytes 49156
  52.3 34.8 %all-to-all-start.1 = ((bf16[2,128,4096]{1,0,2:T(2,128)(2,1)}), bf16[2,128,4096]{1,0,2:T(2,128)(2,1)}, u32[]{:S(2)}, u32[]{:S(2)}) async-start(bf16[2,128,4096]{1,0,2:T(2,128)(2,1)} %copy.47), calls=%async_computation.1 | async-start | bytes 4194304 | tf_op jit(solution)/shard_map/all_to_all | solution.py:38
  56.7 48.9 %reduce-scatter.2.cloned.1.call-start = ((), (), s32[]{:S(2)}) async-start(), calls=%async_computation.4 | async-start | bytes 147456 | tf_op jit(solution)/shard_map/reduce_scatter | solution.py:78
  61.6 1.6 %copy-start.1 = (bf16[2,128,4096]{2,1,0:T(8,128)(2,1)S(1)}, bf16[2,128,4096]{2,1,0:T(8,128)(2,1)}, u32[]{:S(2)}) copy-start(bf16[2,128,4096]{2,1,0:T(8,128)(2,1)} %param.15) | copy-start | bytes 6291460
  93.2 6.1 %copy-start.3 = (f32[16,4]{0,1:T(4,128)S(1)}, f32[16,4]{0,1:T(4,128)}, u32[]{:S(2)}) copy-start(f32[16,4]{0,1:T(4,128)} %param.13) | copy-start | bytes 772
  96.1 9.4 %all-to-all-start.2 = ((bf16[4,2,13,512]{3,1,2,0:T(2,128)(2,1)}), bf16[4,2,13,512]{3,1,2,0:T(2,128)(2,1)S(1)}, u32[]{:S(2)}, u32[]{:S(2)}) async-start(bf16[4,2,13,512]{3,1,2,0:T(2,128)(2,1)} %copy.51), calls=%async_computation.2 | async-start | bytes 212992 | tf_op jit(solution)/shard_map/all_to_all | solution.py:81
Sparse Core Ops, SparseCore 0:
  61.7 33.0 reduce-scatter.1
where the time goes:
time: 115 us; the launch traced here: 114 us
  blocking collectives  33.8 us (29%)
  waiting for transfers between devices  21.8 us (19%)
  local copies, waits for them, and re-layouts  17.5 us (15%)
  between operations  13.5 us (12%)
  starting transfers between devices  12.6 us (11%)
  matrix products  12.1 us (11%)
  other arithmetic  2.59 us (2%)
    all_gather x1, blocking collectives, per_device(): inner_whole = lax.all_gather(inner_vals, 'tp', axis=3, tiled=True)  22.9 us
    all_to_all x1, waiting for transfers between devices, per_device(): lax.all_to_all(packed, 'ep', split_axis=0, concat_axis=0, tiled=True)  15.8 us
    all_gather x1, blocking collectives, per_device(): gathered = lax.all_gather(hidden, 'tp', axis=1, tiled=True)  10.9 us
    unnamed x9, local copies, waits for them, and re-layouts  6.96 us
    all_to_all x1, local copies, waits for them, and re-layouts, per_device(): lax.all_to_all(down_weight, 'tp', split_axis=2, concat_axis=1, tiled=True)  6.15 us
    all_to_all x1, waiting for transfers between devices, per_device(): lax.all_to_all(answers, 'ep', split_axis=0, concat_axis=0, tiled=True)  5.96 us
    all_to_all x1, starting transfers between devices, per_device(): lax.all_to_all(packed, 'ep', split_axis=0, concat_axis=0, tiled=True)  4.87 us
    all_to_all x1, starting transfers between devices, per_device(): lax.all_to_all(down_weight, 'tp', split_axis=2, concat_axis=1, tiled=True)  4.34 us
  transfers between devices with their start and end apart: 4, of which 2 were waited for; matrix products, arithmetic and copies ran while one was open for 19% of the time, Pallas kernels for 0%

commit v1 on v0

--- a/solution.py
+++ b/solution.py
@@ -35,7 +35,10 @@
     shared_down,
 ):
     width_group = lax.axis_size("tp")
-    down_local = lax.all_to_all(down_weight, "tp", split_axis=2, concat_axis=1, tiled=True)
+    down_local = jnp.concatenate(
+        lax.all_to_all(jnp.stack(jnp.split(down_weight, lax.axis_size("tp"), axis=2)), "tp", 0, 0),
+        axis=1,
+    )
     gathered = lax.all_gather(hidden, "tp", axis=1, tiled=True)
     normed = norm_rows(gathered, norm_gain)
     tok_rows, top_count = routes.shape

time: 115 us -> 109 us (0.948)
  waiting for transfers between devices: 21.8 us -> 14.6 us
    all_to_all x1, waiting for transfers between devices: 15.8 us -> 8.61 us  [per_device(): lax.all_to_all(packed, 'ep', split_axis=0, concat_axis=0, tiled=True)]
    all_to_all x1 -> x0, local copies, waits for them, and re-layouts: 6.15 us -> none  [per_device(): lax.all_to_all(down_weight, 'tp', split_axis=2, concat_axis=1, tiled=True)]
    unnamed x9 -> x15, local copies, waits for them, and re-layouts: 6.96 us -> 12.5 us
    another operation x0 -> x1, local copies, waits for them, and re-layouts: none -> 1.68 us  [per_device(): jnp.stack(jnp.split(down_weight, lax.axis_size('tp'), axis=2))]
  transfers between devices with their start and end apart: 4 -> 4, of which waited for: 2 -> 2; matrix products, arithmetic and copies ran while one was open for 19% -> 21% of each run, Pallas kernels for 0% -> 0%
where the time goes in v1:
time: 109 us; the launch traced here: 108 us
  blocking collectives  33.8 us (31%)
  local copies, waits for them, and re-layouts  18.6 us (17%)
  waiting for transfers between devices  14.6 us (13%)
  between operations  13.5 us (12%)
  starting transfers between devices  12.6 us (12%)
  matrix products  12.1 us (11%)
  other arithmetic  2.59 us (2%)
    all_gather x1, blocking collectives, per_device(): inner_whole = lax.all_gather(inner_vals, 'tp', axis=3, tiled=True)  22.9 us
    unnamed x15, local copies, waits for them, and re-layouts  12.5 us
    all_gather x1, blocking collectives, per_device(): gathered = lax.all_gather(hidden, 'tp', axis=1, tiled=True)  10.9 us
    all_to_all x1, waiting for transfers between devices, per_device(): lax.all_to_all(packed, 'ep', split_axis=0, concat_axis=0, tiled=True)  8.61 us
    all_to_all x1, waiting for transfers between devices, per_device(): lax.all_to_all(answers, 'ep', split_axis=0, concat_axis=0, tiled=True)  5.97 us
    all_to_all x1, starting transfers between devices, per_device(): lax.all_to_all(packed, 'ep', split_axis=0, concat_axis=0, tiled=True)  4.87 us
    all_to_all x1, starting transfers between devices, per_device(): lax.all_to_all(jnp.stack(jnp.split(down_weight, lax.axis_size('tp'), axis...  4.34 us
    all_to_all x1, starting transfers between devices, per_device(): lax.all_to_all(answers, 'ep', split_axis=0, concat_axis=0, tiled=True)  3.31 us
  transfers between devices with their start and end apart: 4, of which 2 were waited for; matrix products, arithmetic and copies ran while one was open for 21% of the time, Pallas kernels for 0%

profile of v1, /device:TPU:0, one launch (start us, length us, event | category | flops | bytes accessed | tf_op | source)
XLA Modules:
  0.0 107.7 jit_solution(12991265294327348621)
XLA Ops:
  6.5 0.0 copy-start
  6.5 0.8 convert_reduce_fusion
  7.4 0.1 copy.36
  7.5 0.1 copy.38
  7.6 0.7 select_reduce_fusion.1
  8.3 0.7 multiply_add_fusion
  9.0 0.1 fusion.34
  9.0 10.9 %all_gather.6 = bf16[16,4096]{1,0:T(8,128)(2,1)S(1)} all-gather(bf16[16,512]{1,0:T(8,128)(2,1)} %param.10), channel_id=1, replica_groups=mesh['ep'=4,'tp'=8] {'tp'}, dimensions={1}, use_global_device_ids=true | all-gather | bytes 147456 | tf_op jit(solution)/shard_map/all_gather | solution.py:42
  19.9 0.1 fusion.29
  20.1 2.1 %convolution_convert_fusion = bf16[104,4096]{1,0:T(8,128)(2,1)} fusion(bf16[104,16]{0,1:T(8,128)(2,1)S(1)} %fusion.34, bf16[16,4096]{1,0:T(8,128)(2,1)S(1)} %all_gather.6, f32[4096]{0:T(1024)} %param.11, f32[16]{0:T(128)S(1)} %add_rsqrt_fusion), kind=kOutput, calls=%fused_computation | convolution fusion | flops 14319616 | bytes 1002816 | tf_op jit(solution)/shard_map/dot_general | solution.py:57
  22.2 1.4 %reshape.35 = bf16[4,2,13,4096]{3,2,1,0:T(8,128)(2,1)S(1)} reshape(bf16[104,4096]{1,0:T(8,128)(2,1)} %convolution_convert_fusion) | data formatting | bytes 1703936 | tf_op jit(solution)/shard_map/reshape | solution.py:58
  23.6 1.8 %copy.40 = bf16[4,2,13,4096]{3,1,2,0:T(2,128)(2,1)} copy(bf16[4,2,13,4096]{3,2,1,0:T(8,128)(2,1)S(1)} %reshape.35) | data formatting | bytes 1703936 | tf_op jit(solution)/shard_map/reshape | solution.py:58
  25.4 4.9 %all-to-all-start.1 = ((bf16[4,2,13,4096]{3,1,2,0:T(2,128)(2,1)}), bf16[4,2,13,4096]{3,1,2,0:T(2,128)(2,1)S(1)}, u32[]{:S(2)}, u32[]{:S(2)}) async-start(bf16[4,2,13,4096]{3,1,2,0:T(2,128)(2,1)} %copy.40), calls=%async_computation.1 | async-start | bytes 1703936 | tf_op jit(solution)/shard_map/all_to_all | solution.py:59
  30.3 1.7 %bitcast_dynamic-update-slice_fusion.7 = bf16[8,2,128,512]{3,2,1,0:T(8,128)(2,1)} fusion(bf16[2,128,4096]{2,1,0:T(8,128)(2,1)} %param.16), kind=kLoop, calls=%fused_computation.34 | loop fusion | bytes 524288
  32.0 1.7 %bitcast_dynamic-update-slice_fusion.6 = bf16[8,2,128,512]{3,2,1,0:T(8,128)(2,1)} fusion(bf16[8,2,128,512]{3,2,1,0:T(8,128)(2,1)} %bitcast_dynamic-update-slice_fusion.7, bf16[2,128,4096]{2,1,0:T(8,128)(2,1)} %param.16), kind=kLoop, calls=%fused_computation.33 | loop fusion | bytes 524288
  33.7 1.7 %bitcast_dynamic-update-slice_fusion.5 = bf16[8,2,128,512]{3,2,1,0:T(8,128)(2,1)} fusion(bf16[8,2,128,512]{3,2,1,0:T(8,128)(2,1)} %bitcast_dynamic-update-slice_fusion.6, bf16[2,128,4096]{2,1,0:T(8,128)(2,1)} %param.16), kind=kLoop, calls=%fused_computation.32 | loop fusion | bytes 524288
  35.3 1.7 %bitcast_dynamic-update-slice_fusion.4 = bf16[8,2,128,512]{3,2,1,0:T(8,128)(2,1)} fusion(bf16[8,2,128,512]{3,2,1,0:T(8,128)(2,1)} %bitcast_dynamic-update-slice_fusion.5, bf16[2,128,4096]{2,1,0:T(8,128)(2,1)} %param.16), kind=kLoop, calls=%fused_computation.31 | loop fusion | bytes 524288
  37.0 1.7 %bitcast_dynamic-update-slice_fusion.3 = bf16[8,2,128,512]{3,2,1,0:T(8,128)(2,1)} fusion(bf16[8,2,128,512]{3,2,1,0:T(8,128)(2,1)} %bitcast_dynamic-update-slice_fusion.4, bf16[2,128,4096]{2,1,0:T(8,128)(2,1)} %param.16), kind=kLoop, calls=%fused_computation.30 | loop fusion | bytes 524288
  38.7 1.7 %bitcast_dynamic-update-slice_fusion.2 = bf16[8,2,128,512]{3,2,1,0:T(8,128)(2,1)} fusion(bf16[8,2,128,512]{3,2,1,0:T(8,128)(2,1)} %bitcast_dynamic-update-slice_fusion.3, bf16[2,128,4096]{2,1,0:T(8,128)(2,1)} %param.16), kind=kLoop, calls=%fused_computation.29 | loop fusion | bytes 524288
  40.4 1.7 %bitcast_dynamic-update-slice_fusion.1 = bf16[8,2,128,512]{3,2,1,0:T(8,128)(2,1)} fusion(bf16[8,2,128,512]{3,2,1,0:T(8,128)(2,1)} %bitcast_dynamic-update-slice_fusion.2, bf16[2,128,4096]{2,1,0:T(8,128)(2,1)} %param.16), kind=kLoop, calls=%fused_computation.28 | loop fusion | bytes 524288
  42.0 1.7 %bitcast_dynamic-update-slice_fusion = bf16[8,2,128,512]{3,2,1,0:T(8,128)(2,1)} fusion(bf16[8,2,128,512]{3,2,1,0:T(8,128)(2,1)} %bitcast_dynamic-update-slice_fusion.1, bf16[2,128,4096]{2,1,0:T(8,128)(2,1)} %param.16), kind=kLoop, calls=%fused_computation.27 | loop fusion | bytes 524288 | tf_op jit(solution)/shard_map/stack | solution.py:39
  43.7 0.0 copy-start.2
  43.7 8.6 %all-to-all-done.1 = bf16[4,2,13,4096]{3,1,2,0:T(2,128)(2,1)S(1)} async-done(((bf16[4,2,13,4096]{3,1,2,0:T(2,128)(2,1)}), bf16[4,2,13,4096]{3,1,2,0:T(2,128)(2,1)S(1)}, u32[]{:S(2)}, u32[]{:S(2)}) %all-to-all-start.1) | async-done | bytes 852000 | tf_op jit(solution)/shard_map/all_to_all | solution.py:59
  52.3 4.3 %all-to-all-start = ((bf16[8,2,128,512]{3,2,1,0:T(8,128)(2,1)}), bf16[8,2,128,512]{3,2,1,0:T(8,128)(2,1)}, u32[]{:S(2)}, u32[]{:S(2)}) async-start(bf16[8,2,128,512]{3,2,1,0:T(8,128)(2,1)} %bitcast_dynamic-update-slice_fusion), calls=%async_computation | async-start | bytes 4194304 | tf_op jit(solution)/shard_map/all_to_all | solution.py:39
  56.7 0.0 reduce-scatter.2.cloned.1.call-start
  56.7 0.0 copy-done.2
  56.7 1.6 %fusion.44 = f32[16,128]{1,0:T(8,128)S(1)} fusion(bf16[128,4096]{1,0:T(8,128)(2,1)} %param.17, bf16[16,4096]{1,0:T(8,128)(2,1)S(1)} %all_gather.6, f32[4096]{0:T(1024)S(1)} %copy-done.2, f32[16]{0:T(128)S(1)} %add_rsqrt_fusion), kind=kOutput, calls=%fused_computation.52 | convolution fusion | flops 17039360 | bytes 1204288 | tf_op jit(solution)/shard_map/dot_general | solution.py:66
  58.4 3.1 %convolution_convert_fusion.1 = bf16[16,4096]{1,0:T(8,128)(2,1)} fusion(bf16[128,4096]{1,0:T(8,128)(2,1)} %param.19, bf16[128,4096]{1,0:T(8,128)(2,1)} %param.18, f32[16,128]{1,0:T(8,128)S(1)} %fusion.44, bf16[16,4096]{1,0:T(8,128)(2,1)S(1)} %all_gather.6, f32[4096]{0:T(1024)S(1)} %copy-done.2, f32[16]{0:T(128)S(1)} %add_rsqrt_fusion), kind=kOutput, calls=%fused_computation.1 | convolution fusion | flops 33894400 | bytes 2383936 | tf_op jit(solution)/shard_map/dot_general | solution.py:69
  61.5 0.0 reduce-scatter.2.cloned.1.call-update
  61.5 0.0 copy-done
  61.6 0.0 copy-start.1
  61.6 0.8 fusion.13
  62.4 0.7 copy-done.1
  63.1 0.9 fusion.22
  64.0 22.9 %all_gather.7 = bf16[4,2,13,1024]{3,2,0,1:T(8,128)(2,1)S(1)} all-gather(bf16[4,2,13,128]{3,2,0,1:T(8,128)(2,1)S(1)} %fusion.22), channel_id=1, replica_groups=mesh['ep'=4,'tp'=8] {'tp'}, dimensions={3}, use_global_device_ids=true | all-gather | bytes 239616 | tf_op jit(solution)/shard_map/all_gather | solution.py:72
  86.9 0.2 reshape.41
  87.1 0.0 copy-start.3
  87.1 0.0 all-to-all-done
  87.1 2.1 %fusion.10 = bf16[2,512,4,13]{1,3,2,0:T(8,128)(2,1)S(1)} fusion(bf16[8,2,128,512]{3,2,1,0:T(8,128)(2,1)} %all-to-all-done, bf16[4,2,13,8,128]{4,3,2,0,1:T(8,128)(2,1)S(1)} %reshape.41), kind=kOutput, calls=%fused_computation.10 | convolution fusion | flops 109850624 | bytes 2416640 | tf_op jit(solution)/shard_map/secpf,epfd->secpd/dot_general | solution.py:77
  89.2 0.8 copy.45
  89.9 3.3 %all-to-all-start.2 = ((bf16[4,2,13,512]{3,1,2,0:T(2,128)(2,1)}), bf16[4,2,13,512]{3,1,2,0:T(2,128)(2,1)S(1)}, u32[]{:S(2)}, u32[]{:S(2)}) async-start(bf16[4,2,13,512]{3,1,2,0:T(2,128)(2,1)} %copy.45), calls=%async_computation.2 | async-start | bytes 212992 | tf_op jit(solution)/shard_map/all_to_all | solution.py:84
  93.2 0.0 copy-done.3
  93.2 0.1 select_reduce_fusion
  93.3 6.0 %all-to-all-done.2 = bf16[4,2,13,512]{3,1,2,0:T(2,128)(2,1)S(1)} async-done(((bf16[4,2,13,512]{3,1,2,0:T(2,128)(2,1)}), bf16[4,2,13,512]{3,1,2,0:T(2,128)(2,1)S(1)}, u32[]{:S(2)}, u32[]{:S(2)}) %all-to-all-start.2) | async-done | bytes 106528 | tf_op jit(solution)/shard_map/all_to_all | solution.py:84
  99.3 0.1 reshape.37
  99.4 0.0 reduce-scatter.2.cloned.1.call-done
  99.4 1.5 %fusion.25 = bf16[16,512]{1,0:T(8,128)(2,1)} fusion(f32[16,104]{1,0:T(8,128)S(1)} %select_reduce_fusion, bf16[104,512]{1,0:T(8,128)(2,1)S(1)} %reshape.37, bf16[16,512]{1,0:T(8,128)(2,1)} %reduce-scatter.2.cloned.1.call-done), kind=kOutput, calls=%fused_computation.16 | convolution fusion | flops 10248192 | bytes 145920 | tf_op jit(solution)/shard_map/dot_general | solution.py:86
  (4 shorter events, 0.1 us)
Async XLA Ops:
  6.5 55.0 %copy-start = (bf16[2,128,4096]{2,1,0:T(8,128)(2,1)S(1)}, bf16[2,128,4096]{2,1,0:T(8,128)(2,1)}, u32[]{:S(2)}) copy-start(bf16[2,128,4096]{2,1,0:T(8,128)(2,1)} %param.14) | copy-start | bytes 6291460
  25.4 26.9 %all-to-all-start.1 = ((bf16[4,2,13,4096]{3,1,2,0:T(2,128)(2,1)}), bf16[4,2,13,4096]{3,1,2,0:T(2,128)(2,1)S(1)}, u32[]{:S(2)}, u32[]{:S(2)}) async-start(bf16[4,2,13,4096]{3,1,2,0:T(2,128)(2,1)} %copy.40), calls=%async_computation.1 | async-start | bytes 1703936 | tf_op jit(solution)/shard_map/all_to_all | solution.py:59
  43.7 13.0 %copy-start.2 = (f32[4096]{0:T(1024)S(1)}, f32[4096]{0:T(1024)}, u32[]{:S(2)}) copy-start(f32[4096]{0:T(1024)} %param.11) | copy-start | bytes 49156
  52.3 34.8 %all-to-all-start = ((bf16[8,2,128,512]{3,2,1,0:T(8,128)(2,1)}), bf16[8,2,128,512]{3,2,1,0:T(8,128)(2,1)}, u32[]{:S(2)}, u32[]{:S(2)}) async-start(bf16[8,2,128,512]{3,2,1,0:T(8,128)(2,1)} %bitcast_dynamic-update-slice_fusion), calls=%async_computation | async-start | bytes 4194304 | tf_op jit(solution)/shard_map/all_to_all | solution.py:39
  56.7 42.7 %reduce-scatter.2.cloned.1.call-start = ((), (), s32[]{:S(2)}) async-start(), calls=%async_computation.4 | async-start | bytes 147456 | tf_op jit(solution)/shard_map/reduce_scatter | solution.py:81
  61.6 1.6 %copy-start.1 = (bf16[2,128,4096]{2,1,0:T(8,128)(2,1)S(1)}, bf16[2,128,4096]{2,1,0:T(8,128)(2,1)}, u32[]{:S(2)}) copy-start(bf16[2,128,4096]{2,1,0:T(8,128)(2,1)} %param.15) | copy-start | bytes 6291460
  87.1 6.2 %copy-start.3 = (f32[16,4]{0,1:T(4,128)S(1)}, f32[16,4]{0,1:T(4,128)}, u32[]{:S(2)}) copy-start(f32[16,4]{0,1:T(4,128)} %param.13) | copy-start | bytes 772
  89.9 9.4 %all-to-all-start.2 = ((bf16[4,2,13,512]{3,1,2,0:T(2,128)(2,1)}), bf16[4,2,13,512]{3,1,2,0:T(2,128)(2,1)S(1)}, u32[]{:S(2)}, u32[]{:S(2)}) async-start(bf16[4,2,13,512]{3,1,2,0:T(2,128)(2,1)} %copy.45), calls=%async_computation.2 | async-start | bytes 212992 | tf_op jit(solution)/shard_map/all_to_all | solution.py:84
Sparse Core Ops, SparseCore 0:
  61.7 33.0 reduce-scatter.1
